TPU v7x, 32 devices: a whole 2x2x4 slice. The times are simulated.
32 devices in a mesh: sp: 16 (over z, y, core), tp: 2 (over x).
Axes of the slice: x: 2, y: 2, z: 4, core: 2. Of those that a mesh axis runs over, the one named last changes fastest.
Arguments:
- resid: bfloat16 [4096, 2048], P('sp', 'tp'), may hold values from -80 to 80, as said below
- norm_gain: float32 [2, 2048], P(None, 'tp'), may hold values from 0.1 to 1.9
- w_in: bfloat16 [2, 2048, 1024], P(None, 'tp', 'sp'), may hold values from -0.125 to 0.125
- w_pool: bfloat16 [2, 4, 256, 256], P(None, 'tp'), may hold values from -0.375 to 0.375
- pool_scale: float32 [2, 1024], P(None, 'tp'), may hold values from 0.1 to 1.9
- w_out: bfloat16 [2, 1024, 2048], P(None, 'sp', 'tp'), may hold values from -0.1875 to 0.1875
- final_gain: float32 [2048], P('tp'), may hold values from 0.1 to 1.9
Outputs:
- normed: bfloat16 [4096, 2048], P('sp', 'tp')
Inputs may be any that keep to these rules, and one draw needn't show every extreme that they name: `resid`: Real-valued entries of order 0.1 to ten.
All inputs are finite; a program needn't handle non-finite values.
Results may differ from a plain program's by a relative error of at most 0.015.
Values may be sent and summed in bfloat16 or wider, within the bound.
A program may use at most 64 MiB of HBM per device.

v0:
```python
import jax
import jax.numpy as jnp
from jax import lax
from jax.sharding import PartitionSpec as P

LAYERS = 2


margin = 8
eps = 1e-06


def padded_2(value, sides, width):
    for axis, dim in sides:
        count, length = (lax.axis_size(axis), value.shape[dim])
        up = [(i, (i + 1) % count) for i in range(count - 1)]
        down = [(j, i) for i, j in up]
        last = lax.slice_in_dim(value, length - width, length, axis=dim)
        initial = lax.slice_in_dim(value, 0, width, axis=dim)
        before = lax.ppermute(last, axis, up)
        after = lax.ppermute(initial, axis, down)
        value = jnp.concatenate([before, value, after], axis=dim)
    return value


def nested_sums(padded, count_rows):
    total = padded[margin - 1 : margin - 1 + count_rows] + padded[margin : margin + count_rows]
    sums = [total]
    for level in range(1, 4):
        half = 2**level
        for offset in range(half // 2 + 1, half + 1):
            total = total + padded[margin - offset : margin - offset + count_rows]
        for offset in range(half // 2, half):
            total = total + padded[margin + offset : margin + offset + count_rows]
        sums.append(total)
    return sums


def window_count(where, seq_len, level):
    left = 2**level
    right = 2**level - 1
    upper = jnp.clip(where + right + 1, 0, seq_len)
    lower = jnp.clip(where - left, 0, seq_len)
    return (upper - lower).astype(jnp.float32)


def scaled(xf, gain, width):
    squares = lax.psum(jnp.sum(xf * xf, axis=1), "tp")
    return (xf * lax.rsqrt(squares / width + eps)[:, None] * gain[None, :]).astype(jnp.bfloat16)


def shards(resid, norm_gain, w_in, w_pool, pool_scale, w_out, final_gain):
    tok_rows = resid.shape[0]
    blocks_tp = lax.axis_size("tp")
    width = blocks_tp * resid.shape[1]
    channels = w_pool.shape[1] * w_pool.shape[2]
    groups_here = w_pool.shape[1]
    group_width = w_pool.shape[2]
    seq_len = tok_rows * lax.axis_size("sp")
    where = lax.axis_index("sp") * tok_rows + jnp.arange(tok_rows, dtype=jnp.int32)
    group_ids = (
        lax.axis_index("tp") * groups_here + jnp.arange(channels, dtype=jnp.int32) // group_width
    )
    all_in, all_out = (
        lax.all_gather(w_in, "sp", axis=2, tiled=True),
        lax.all_gather(w_out, "sp", axis=1, tiled=True),
    )
    xf = resid.astype(jnp.float32)
    for layer in range(LAYERS):
        own_hidden = scaled(xf, norm_gain[layer], width)
        in_block = all_in[layer]
        partial_value = jnp.dot(own_hidden, in_block, preferred_element_type=jnp.float32).astype(
            jnp.bfloat16
        )
        upward = (
            lax.psum_scatter(partial_value, "tp", scatter_dimension=1, tiled=True)
            .astype(jnp.float32)
            .astype(jnp.bfloat16)
        )
        padded = padded_2(upward, (("sp", 0),), margin).astype(jnp.float32)
        sums = nested_sums(padded, tok_rows)
        wsum = sums[0]
        counted = jnp.broadcast_to(window_count(where, seq_len, 0)[:, None], (tok_rows, channels))
        for level in range(1, 4):
            chosen = (group_ids == level)[None, :]
            wsum = jnp.where(chosen, sums[level], wsum)
            counted = jnp.where(chosen, window_count(where, seq_len, level)[:, None], counted)
        pooled = (wsum / counted - upward.astype(jnp.float32)).astype(jnp.bfloat16)
        mapped = jnp.einsum(
            "tgc,gcd->tgd",
            pooled.reshape(tok_rows, groups_here, group_width),
            w_pool[layer],
            preferred_element_type=jnp.float32,
        )
        mixed = (mapped.reshape(tok_rows, channels) * pool_scale[layer][None, :]).astype(
            jnp.bfloat16
        )
        mixed_all = lax.all_gather(mixed, "tp", axis=1, tiled=True)
        output = jnp.dot(mixed_all, all_out[layer], preferred_element_type=jnp.float32)
        stored = (xf + output).astype(jnp.bfloat16)
        stored = lax.optimization_barrier(stored)
        xf = stored.astype(jnp.float32)
    return scaled(xf, final_gain, width)


def solution(mesh):
    placed = (
        P("sp", "tp"),
        P(None, "tp"),
        P(None, "tp", "sp"),
        P(None, "tp", None, None),
        P(None, "tp"),
        P(None, "sp", "tp"),
        P("tp"),
    )
    return jax.shard_map(
        shards, mesh=mesh, in_specs=placed, out_specs=P("sp", "tp"), check_vma=False
    )
```

profile of v0, /device:TPU:0, one launch (start us, length us, event | category | flops | bytes accessed | tf_op | source)
XLA Modules:
  0.0 188.0 jit_solution(12164840678159119583)
XLA Ops:
  6.5 0.0 copy-start.3
  6.5 0.0 all-gather.3.cloned.1.call-start
  6.5 0.7 all-gather.3.cloned.1.call-update
  7.3 0.0 reduce-scatter.3.cloned.1.call-start
  7.3 1.2 fusion.11
  8.5 5.9 %psum.21 = f32[256]{0:T(256)S(1)} all-reduce(f32[256]{0:T(256)S(1)} %fusion.11), channel_id=1, replica_groups=mesh['sp'=16,'tp'=2] {'tp'}, use_global_device_ids=true, to_apply=%region_1.2 | all-reduce | flops 256 | bytes 2048 | tf_op jit(solution)/shard_map/psum | solution.py:48
  14.4 0.8 fusion.49
  15.2 47.5 %all-gather.3.cloned.1.call-done = bf16[2,1024,1024]{1,2,0:T(8,128)(2,1)} async-done(((bf16[2,1024,64]{1,2,0:T(8,128)(2,1)}), bf16[2,1024,1024]{1,2,0:T(8,128)(2,1)}) %all-gather.3.cloned.1.call-update) | async-done | bytes 4194320 | tf_op jit(solution)/shard_map/all_gather | solution.py:65
  62.7 3.3 %fusion.6 = bf16[256,1024]{1,0:T(8,128)(2,1)} fusion(bf16[2,1024,1024]{1,2,0:T(8,128)(2,1)} %all-gather.3.cloned.1.call-done, bf16[256,1024]{1,0:T(8,128)(2,1)} %param.7, f32[1024]{0:T(1024)S(1)} %bitcast.63, f32[256]{0:T(256)S(1)} %add_rsqrt_fusion.2), kind=kOutput, calls=%fused_computation.18 | convolution fusion | flops 538181632 | bytes 3150848 | tf_op jit(solution)/shard_map/dot_general | solution.py:72
  66.0 0.0 reduce-scatter.3.cloned.1.call-update
  66.0 0.0 all-gather.5.cloned.1.call-start
  66.1 0.7 all-gather.5.cloned.1.call-update
  66.8 0.0 reduce-scatter.5.cloned.1.call-start
  66.9 0.0 copy-done.3
  66.9 12.5 %reduce-scatter.3.cloned.1.call-done = bf16[256,512]{1,0:T(8,128)(2,1)} async-done(((bf16[256,1024]{1,0:T(8,128)(2,1)}), bf16[256,512]{1,0:T(8,128)(2,1)}) %reduce-scatter.3.cloned.1.call-update) | async-done | bytes 262160 | tf_op jit(solution)/shard_map/reduce_scatter | solution.py:76
  79.3 0.7 fusion.48
  80.1 1.6 collective-permute-start
  81.6 1.3 collective-permute-start.1
  82.9 0.0 collective-permute-done
  83.0 3.2 %collective-permute-done.1 = bf16[8,512]{1,0:T(8,128)(2,1)S(1)} collective-permute-done((bf16[8,512]{1,0:T(8,128)(2,1)S(1)}, bf16[8,512]{1,0:T(8,128)(2,1)S(1)}, u32[]{:S(2)}, u32[]{:S(2)}) %collective-permute-start.1) | collective-permute-done | bytes 8224 | tf_op jit(solution)/shard_map/ppermute | solution.py:21
  86.1 1.0 maximum_convert_fusion
  87.1 0.0 copy-start.1
  87.1 0.0 copy-start
  87.2 2.0 %fusion.31 = bf16[256,512]{1,0:T(8,128)(2,1)S(1)} fusion(bf16[256,512]{1,0:T(8,128)(2,1)} %reduce-scatter.3.cloned.1.call-done, f32[272,512]{1,0:T(8,128)S(1)} %maximum_convert_fusion, f32[256]{0:T(256)S(1)} %get-tuple-element.13, f32[256]{0:T(256)S(1)} %get-tuple-element.14, f32[256]{0:T(256)S(1)} %get-tuple-element.15, f32[256]{0:T(256)S(1)} %get-tuple-element.16, ...), kind=kLoop, calls=%fused_computation.74 | loop fusion | flops 3276800 | bytes 8918528 | tf_op jit(solution)/shard_map/convert_element_type | solution.py:88
  89.2 0.0 copy-done.1
  89.2 0.3 fusion.36
  89.5 0.1 fusion.26
  89.6 8.4 %all_gather.13 = bf16[256,1024]{0,1:T(8,128)(2,1)S(1)} all-gather(bf16[256,512]{0,1:T(8,128)(2,1)S(1)} %fusion.26), channel_id=1, replica_groups=mesh['sp'=16,'tp'=2] {'tp'}, dimensions={1}, use_global_device_ids=true | all-gather | bytes 786432 | tf_op jit(solution)/shard_map/all_gather | solution.py:98
  98.0 34.0 %all-gather.5.cloned.1.call-done = bf16[2,1024,1024]{2,1,0:T(8,128)(2,1)} async-done(((bf16[2,64,1024]{2,1,0:T(8,128)(2,1)}), bf16[2,1024,1024]{2,1,0:T(8,128)(2,1)}) %all-gather.5.cloned.1.call-update) | async-done | bytes 4194320 | tf_op jit(solution)/shard_map/all_gather | solution.py:66
  132.0 0.0 copy-done
  132.0 2.3 %fusion.4 = bf16[256,1024]{1,0:T(8,128)(2,1)S(1)} fusion(bf16[256,1024]{0,1:T(8,128)(2,1)S(1)} %all_gather.13, bf16[2,1024,1024]{2,1,0:T(8,128)(2,1)} %all-gather.5.cloned.1.call-done, bf16[256,1024]{1,0:T(8,128)(2,1)S(1)} %copy-done), kind=kOutput, calls=%fused_computation.16 | convolution fusion | flops 537657344 | bytes 3670016 | tf_op jit(solution)/shard_map/dot_general | solution.py:99
  134.3 0.2 fusion.14
  134.5 4.9 %psum.22 = f32[256]{0:T(256)S(1)} all-reduce(f32[256]{0:T(256)S(1)} %fusion.14), channel_id=1, replica_groups=mesh['sp'=16,'tp'=2] {'tp'}, use_global_device_ids=true, to_apply=%region_4.5 | all-reduce | flops 256 | bytes 2048 | tf_op jit(solution)/shard_map/psum | solution.py:48
  139.4 3.2 %fusion.7 = bf16[256,1024]{1,0:T(8,128)(2,1)} fusion(bf16[2,1024,1024]{1,2,0:T(8,128)(2,1)} %all-gather.3.cloned.1.call-done, bf16[256,1024]{1,0:T(8,128)(2,1)S(1)} %fusion.4, f32[1024]{0:T(1024)S(1)} %bitcast.62, f32[256]{0:T(256)S(1)} %add_rsqrt_fusion.1), kind=kOutput, calls=%fused_computation.19 | convolution fusion | flops 538181632 | bytes 3150848 | tf_op jit(solution)/shard_map/dot_general | solution.py:72
  142.6 0.0 reduce-scatter.5.cloned.1.call-update
  142.6 13.3 %reduce-scatter.5.cloned.1.call-done = bf16[256,512]{1,0:T(8,128)(2,1)} async-done(((bf16[256,1024]{1,0:T(8,128)(2,1)}), bf16[256,512]{1,0:T(8,128)(2,1)}) %reduce-scatter.5.cloned.1.call-update) | async-done | bytes 262160 | tf_op jit(solution)/shard_map/reduce_scatter | solution.py:76
  155.9 0.7 fusion.47
  156.6 1.6 collective-permute-start.2
  158.2 1.3 collective-permute-start.3
  159.5 0.0 collective-permute-done.2
  159.5 3.2 %collective-permute-done.3 = bf16[8,512]{1,0:T(8,128)(2,1)S(1)} collective-permute-done((bf16[8,512]{1,0:T(8,128)(2,1)S(1)}, bf16[8,512]{1,0:T(8,128)(2,1)S(1)}, u32[]{:S(2)}, u32[]{:S(2)}) %collective-permute-start.3) | collective-permute-done | bytes 8224 | tf_op jit(solution)/shard_map/ppermute | solution.py:21
  162.7 1.0 maximum_convert_fusion.1
  163.7 0.0 copy-start.4
  163.7 2.1 %fusion.32 = bf16[256,512]{1,0:T(8,128)(2,1)S(1)} fusion(bf16[256,512]{1,0:T(8,128)(2,1)} %reduce-scatter.5.cloned.1.call-done, f32[272,512]{1,0:T(8,128)S(1)} %maximum_convert_fusion.1, f32[256]{0:T(256)S(1)} %get-tuple-element.13, f32[256]{0:T(256)S(1)} %get-tuple-element.14, f32[256]{0:T(256)S(1)} %get-tuple-element.15, f32[256]{0:T(256)S(1)} %get-tuple-element.16, ...), kind=kLoop, calls=%fused_computation.75 | loop fusion | flops 3276800 | bytes 8918528 | tf_op jit(solution)/shard_map/convert_element_type | solution.py:88
  165.8 0.0 copy-start.2
  165.8 0.3 fusion.33
  166.1 0.1 fusion.25
  166.2 8.4 %all_gather.15 = bf16[256,1024]{0,1:T(8,128)(2,1)S(1)} all-gather(bf16[256,512]{0,1:T(8,128)(2,1)S(1)} %fusion.25), channel_id=1, replica_groups=mesh['sp'=16,'tp'=2] {'tp'}, dimensions={1}, use_global_device_ids=true | all-gather | bytes 786432 | tf_op jit(solution)/shard_map/all_gather | solution.py:98
  174.7 0.0 copy-done.4
  174.7 0.7 fusion.5
  175.4 0.2 fusion.8
  175.6 4.9 %psum.23 = f32[256]{0:T(256)S(1)} all-reduce(f32[256]{0:T(256)S(1)} %fusion.8), channel_id=1, replica_groups=mesh['sp'=16,'tp'=2] {'tp'}, use_global_device_ids=true, to_apply=%region_7.8 | all-reduce | flops 256 | bytes 2048 | tf_op jit(solution)/shard_map/psum | solution.py:48
  180.5 0.0 copy-done.2
  180.5 1.0 fusion.10
  (8 shorter events, 0.1 us)
Async XLA Ops:
  6.5 60.3 %copy-start.3 = (f32[2,512]{1,0:T(2,128)S(1)}, f32[2,512]{1,0:T(2,128)}, u32[]{:S(2)}) copy-start(f32[2,512]{1,0:T(2,128)} %param.11) | copy-start | bytes 12292
  6.5 56.1 %all-gather.3.cloned.1.call-start = ((), (), s32[]{:S(2)}) async-start(), calls=%async_computation.2 | async-start | bytes 4456448 | tf_op jit(solution)/shard_map/all_gather | solution.py:65
  7.3 72.1 %reduce-scatter.3.cloned.1.call-start = ((), (), s32[]{:S(2)}) async-start(), calls=%async_computation.3 | async-start | bytes 786432 | tf_op jit(solution)/shard_map/reduce_scatter | solution.py:76
  66.0 66.0 %all-gather.5.cloned.1.call-start = ((), (), s32[]{:S(2)}) async-start(), calls=%async_computation.4 | async-start | bytes 4456448 | tf_op jit(solution)/shard_map/all_gather | solution.py:66
  66.8 89.2 %reduce-scatter.5.cloned.1.call-start = ((), (), s32[]{:S(2)}) async-start(), calls=%async_computation.5 | async-start | bytes 786432 | tf_op jit(solution)/shard_map/reduce_scatter | solution.py:76
  80.1 2.9 %collective-permute-start = (bf16[8,512]{1,0:T(8,128)(2,1)S(1)}, bf16[8,512]{1,0:T(8,128)(2,1)S(1)}, u32[]{:S(2)}, u32[]{:S(2)}) collective-permute-start(bf16[8,512]{1,0:T(8,128)(2,1)S(1)} %get-tuple-element.7), channel_id=1, source_target_pairs={{0,2},{2,4},{4,6},{6,8},{8,10},{10,12},{12,14},{14,16},{16,18},{18... | collective-permute-start | bytes 24584 | tf_op jit(solution)/shard_map/ppermute | solution.py:20
  81.6 4.5 %collective-permute-start.1 = (bf16[8,512]{1,0:T(8,128)(2,1)S(1)}, bf16[8,512]{1,0:T(8,128)(2,1)S(1)}, u32[]{:S(2)}, u32[]{:S(2)}) collective-permute-start(bf16[8,512]{1,0:T(8,128)(2,1)S(1)} %get-tuple-element.8), channel_id=1, source_target_pairs={{2,0},{4,2},{6,4},{8,6},{10,8},{12,10},{14,12},{16,14},{18,16},{20... | collective-permute-start | bytes 24584 | tf_op jit(solution)/shard_map/ppermute | solution.py:21
  87.1 2.0 %copy-start.1 = (bf16[2,2,256,256]{3,2,1,0:T(8,128)(2,1)S(1)}, bf16[2,2,256,256]{3,2,1,0:T(8,128)(2,1)}, u32[]{:S(2)}) copy-start(bf16[2,2,256,256]{3,2,1,0:T(8,128)(2,1)} %param.10) | copy-start | bytes 1572868
  87.1 44.8 %copy-start = (bf16[256,1024]{1,0:T(8,128)(2,1)S(1)}, bf16[256,1024]{1,0:T(8,128)(2,1)}, u32[]{:S(2)}) copy-start(bf16[256,1024]{1,0:T(8,128)(2,1)} %param.7) | copy-start | bytes 1572868
  156.6 2.9 %collective-permute-start.2 = (bf16[8,512]{1,0:T(8,128)(2,1)S(1)}, bf16[8,512]{1,0:T(8,128)(2,1)S(1)}, u32[]{:S(2)}, u32[]{:S(2)}) collective-permute-start(bf16[8,512]{1,0:T(8,128)(2,1)S(1)} %get-tuple-element.5), channel_id=1, source_target_pairs={{0,2},{2,4},{4,6},{6,8},{8,10},{10,12},{12,14},{14,16},{16,18},{18... | collective-permute-start | bytes 24584 | tf_op jit(solution)/shard_map/ppermute | solution.py:20
  158.2 4.5 %collective-permute-start.3 = (bf16[8,512]{1,0:T(8,128)(2,1)S(1)}, bf16[8,512]{1,0:T(8,128)(2,1)S(1)}, u32[]{:S(2)}, u32[]{:S(2)}) collective-permute-start(bf16[8,512]{1,0:T(8,128)(2,1)S(1)} %get-tuple-element.6), channel_id=1, source_target_pairs={{2,0},{4,2},{6,4},{8,6},{10,8},{12,10},{14,12},{16,14},{18,16},{20... | collective-permute-start | bytes 24584 | tf_op jit(solution)/shard_map/ppermute | solution.py:21
  163.7 10.9 %copy-start.4 = (bf16[2,1024,1024]{2,1,0:T(8,128)(2,1)S(1)}, bf16[2,1024,1024]{2,1,0:T(8,128)(2,1)}, u32[]{:S(2)}) copy-start(bf16[2,1024,1024]{2,1,0:T(8,128)(2,1)} %all-gather.5.cloned.1.call-done) | copy-start | bytes 12582916
  165.8 14.7 %copy-start.2 = (f32[1024]{0:T(1024)S(1)}, f32[1024]{0:T(1024)}, u32[]{:S(2)}) copy-start(f32[1024]{0:T(1024)} %param.13) | copy-start | bytes 12292
Sparse Core Ops, SparseCore 0:
  9.5 53.1 all-gather.2
  66.1 13.1 reduce-scatter.2
  81.5 50.4 all-gather.4
  142.7 13.1 reduce-scatter.4
where the time goes:
time: 190 us; the launch traced here: 188 us
  waiting for transfers between devices  115 us (61%)
  blocking collectives  32.6 us (17%)
  between operations  13.3 us (7%)
  matrix products  10.1 us (5%)
  other arithmetic  9.01 us (5%)
  starting transfers between devices  5.85 us (3%)
  local copies, waits for them, and re-layouts  2.25 us (1%)
    all_gather x1, waiting for transfers between devices, shards(): lax.all_gather(w_in, 'sp', axis=2, tiled=True)  47.5 us
    all_gather x1, waiting for transfers between devices, shards(): lax.all_gather(w_out, 'sp', axis=1, tiled=True)  34 us
    reduce_scatter x2, waiting for transfers between devices, shards(): lax.psum_scatter(partial_value, 'tp', scatter_dimension=1, tiled=True)  25.8 us
    all_gather x2, blocking collectives, shards(): mixed_all = lax.all_gather(mixed, 'tp', axis=1, tiled=True)  16.8 us
    psum x3, blocking collectives, scaled(): squares = lax.psum(jnp.sum(xf * xf, axis=1), 'tp')  15.7 us
    dot_general x2, matrix products, shards(): jnp.dot(own_hidden, in_block, preferred_element_type=jnp.float32)  6.48 us
    ppermute x2, waiting for transfers between devices, padded_2(): after = lax.ppermute(initial, axis, down)  6.35 us
    convert_element_type x2, other arithmetic, shards(): pooled = (wsum / counted - upward.astype(jnp.float32)).astype(jnp.bfloat16)  4.09 us
  transfers between devices with their start and end apart: 8, of which 6 were waited for; matrix products, arithmetic and copies ran while one was open for 3% of the time, Pallas kernels for 0%

commit v1 on v0

--- a/solution.py
+++ b/solution.py
@@ -1,6 +1,10 @@
+import functools
+
 import jax
 import jax.numpy as jnp
 from jax import lax
+from jax.experimental import pallas as pl
+from jax.experimental.pallas import tpu as pltpu
 from jax.sharding import PartitionSpec as P
 
 LAYERS = 2
@@ -103,6 +107,460 @@
     return scaled(xf, final_gain, width)
 
 
+MESH = pl.DeviceIdType.MESH
+
+
+def fused(
+    sp_size,
+    resid_ref,
+    gain_ref,
+    final_ref,
+    own_w,
+    pool_ref,
+    pscale_ref,
+    out_ref,
+    weights,
+    xg,
+    xcur,
+    own_part,
+    acc,
+    part_send,
+    part_recv,
+    uhalo,
+    mix_send,
+    mix_recv,
+    ss_send,
+    ss_recv,
+    w_send_sem,
+    w_recv_sem,
+    x_send_sem,
+    x_recv_sem,
+    h_send_sem,
+    h_recv_sem,
+    s_send_sem,
+    s_recv_sem,
+):
+    depth = sp_size // 4
+    rows = own_w.shape[1]
+    tokens, width_here = resid_ref.shape
+    groups, cg = pool_ref.shape[1], pool_ref.shape[2]
+    half = groups * cg
+    width = 2 * width_here
+    edge = 2 * margin
+    me = lax.axis_index("sp")
+    t = lax.axis_index("tp")
+    peer = 1 - t
+    core = lax.rem(me, 2)
+    y = lax.rem(me // 2, 2)
+    z = me // 4
+
+    def number(zz, yy, cc):
+        return (zz * 2 + yy) * 2 + cc
+
+    sibling = number(z, y, 1 - core)
+    across = number(z, 1 - y, core)
+
+    barrier = pltpu.get_barrier_semaphore()
+
+    def greet(device):
+        pl.semaphore_signal(barrier, inc=1, device_id=device, device_id_type=MESH)
+
+    greet({"sp": sibling})
+    greet({"sp": across})
+    greet({"tp": peer})
+    for ok, who in (
+        (z > 0, me - 4),
+        (z < depth - 1, me + 4),
+        (me > 0, me - 1),
+        (me < sp_size - 1, me + 1),
+    ):
+
+        @pl.when(ok)
+        def _(who=who):
+            greet({"sp": who})
+
+    expected = (
+        3
+        + jnp.where(z > 0, 1, 0)
+        + jnp.where(z < depth - 1, 1, 0)
+        + jnp.where(me > 0, 1, 0)
+        + jnp.where(me < sp_size - 1, 1, 0)
+    )
+    pl.semaphore_wait(barrier, expected)
+
+    def landing(stage, piece):
+        return weights.at[stage, pl.ds(pl.multiple_of(piece * rows, rows), rows), :]
+
+    def hop(stage, zz, yy, way, target, from_own=False):
+        piece = number(zz, yy, core)
+        slot = {"sib": zz * 2 + yy, "y": 2 * depth + zz, "up": 3 * depth + zz, "down": 4 * depth + zz}[way]
+        return pltpu.make_async_remote_copy(
+            src_ref=own_w.at[stage] if from_own else landing(stage, piece),
+            dst_ref=landing(stage, piece),
+            send_sem=w_send_sem.at[stage, slot],
+            recv_sem=w_recv_sem.at[stage, piece],
+            device_id={"sp": target},
+            device_id_type=MESH,
+        )
+
+    def wait_piece(stage, zz, yy, cc):
+        piece = number(zz, yy, cc)
+        pltpu.make_async_remote_copy(
+            src_ref=landing(stage, piece),
+            dst_ref=landing(stage, piece),
+            send_sem=w_send_sem.at[stage, 0],
+            recv_sem=w_recv_sem.at[stage, piece],
+            device_id={"sp": sibling},
+            device_id_type=MESH,
+        ).wait_recv()
+
+    def each_own(stage, act):
+        @pl.when(z < depth - 1)
+        def _():
+            act(hop(stage, z, y, "up", me + 4, True))
+
+        @pl.when(z > 0)
+        def _():
+            act(hop(stage, z, y, "down", me - 4, True))
+
+        act(hop(stage, z, y, "y", across, True))
+        act(hop(stage, z, y, "sib", sibling, True))
+
+    def each_z(stage, d, act, arrive):
+        @pl.when(z - d >= 0)
+        def _():
+            if arrive:
+                wait_piece(stage, z - d, y, core)
+
+            @pl.when(z < depth - 1)
+            def _():
+                act(hop(stage, z - d, y, "up", me + 4))
+
+            act(hop(stage, z - d, y, "y", across))
+            act(hop(stage, z - d, y, "sib", sibling))
+
+        @pl.when(z + d < depth)
+        def _():
+            if arrive:
+                wait_piece(stage, z + d, y, core)
+
+            @pl.when(z > 0)
+            def _():
+                act(hop(stage, z + d, y, "down", me - 4))
+
+            act(hop(stage, z + d, y, "y", across))
+            act(hop(stage, z + d, y, "sib", sibling))
+
+    def each_y(stage, d, act, arrive):
+        def one(zz):
+            if arrive:
+                wait_piece(stage, zz, 1 - y, core)
+            act(hop(stage, zz, 1 - y, "sib", sibling))
+
+        if d == 0:
+            one(z)
+        else:
+
+            @pl.when(z - d >= 0)
+            def _():
+                one(z - d)
+
+            @pl.when(z + d < depth)
+            def _():
+                one(z + d)
+
+    begin = lambda copy: copy.start()
+    drain = lambda copy: copy.wait_send()
+
+    def process(stage):
+        for d in range(1, depth):
+            each_z(stage, d, begin, True)
+            if d == depth - 1 and stage + 1 < 2 * LAYERS:
+                each_own(stage + 1, begin)
+            each_y(stage, d - 1, begin, True)
+        each_y(stage, depth - 1, begin, True)
+
+    def settle(stage):
+        for zz in range(depth):
+            for yy in range(2):
+                wait_piece(stage, zz, yy, 1 - core)
+
+    def finish(stage):
+        each_own(stage, drain)
+        for d in range(1, depth):
+            each_z(stage, d, drain, False)
+        for d in range(depth):
+            each_y(stage, d, drain, False)
+
+    diagonal = lax.broadcasted_iota(jnp.int32, (tokens, tokens), 0) == lax.broadcasted_iota(
+        jnp.int32, (tokens, tokens), 1
+    )
+
+    def send_squares(k):
+        return pltpu.make_async_remote_copy(
+            src_ref=ss_send.at[k],
+            dst_ref=ss_recv.at[k],
+            send_sem=s_send_sem.at[k],
+            recv_sem=s_recv_sem.at[k],
+            device_id={"tp": peer},
+            device_id_type=MESH,
+        )
+
+    def store_squares(k, column):
+        line = jnp.sum(jnp.where(diagonal, column, 0.0), axis=0, keepdims=True)
+        ss_send[k] = jnp.broadcast_to(line, ss_send.shape[1:])
+
+    def norm_factor(k):
+        send_squares(k).wait_recv()
+        line = ss_send[k][0:1, :] + ss_recv[k][0:1, :]
+        column = jnp.sum(jnp.where(diagonal, line, 0.0), axis=1, keepdims=True)
+        return lax.rsqrt(column / width + eps)
+
+    def x_copy(kind, layer, j):
+        k = (kind * LAYERS + layer) * groups + j
+        source, target = ((part_send, part_recv), (mix_send, mix_recv))[kind]
+        return pltpu.make_async_remote_copy(
+            src_ref=source.at[layer, j],
+            dst_ref=target.at[layer, j],
+            send_sem=x_send_sem.at[k],
+            recv_sem=x_recv_sem.at[k],
+            device_id={"tp": peer},
+            device_id_type=MESH,
+        )
+
+    def halo(layer, upward):
+        if upward:
+            source = uhalo.at[layer, pl.ds(tokens, edge), :]
+            target = uhalo.at[layer, pl.ds(0, edge), :]
+        else:
+            source = uhalo.at[layer, pl.ds(edge, edge), :]
+            target = uhalo.at[layer, pl.ds(edge + tokens, edge), :]
+        k = layer * 2 + (1 if upward else 0)
+        return pltpu.make_async_remote_copy(
+            src_ref=source,
+            dst_ref=target,
+            send_sem=h_send_sem.at[k],
+            recv_sem=h_recv_sem.at[k],
+            device_id={"sp": me + 1 if upward else me - 1},
+            device_id_type=MESH,
+        )
+
+    def project(layer, which, j):
+        start = pl.multiple_of(which * half + j * cg, cg)
+        block = weights[2 * layer, pl.ds(start, cg), :]
+        return lax.dot_general(
+            xg[...], block, (((1,), (1,)), ((), ())), preferred_element_type=jnp.float32
+        )
+
+    def inward(layer):
+        for j in range(groups):
+            part_send[layer, j] = project(layer, peer, j).astype(jnp.bfloat16)
+        for j in range(groups):
+            x_copy(0, layer, j).start()
+            own_part[:, j * cg : (j + 1) * cg] = project(layer, t, j)
+
+    def pooling(layer):
+        factor = norm_factor(layer)
+        for j in range(groups):
+            x_copy(0, layer, j).wait_recv()
+            value = own_part[:, j * cg : (j + 1) * cg] + part_recv[layer, j].astype(jnp.float32)
+            uhalo[layer, pl.ds(edge, tokens), j * cg : (j + 1) * cg] = (value * factor).astype(
+                jnp.bfloat16
+            )
+        row = lax.broadcasted_iota(jnp.int32, (tokens, tokens + 2 * edge), 0)
+        col = lax.broadcasted_iota(jnp.int32, (tokens, tokens + 2 * edge), 1) - edge
+        where = me * tokens + lax.broadcasted_iota(jnp.int32, (tokens, 1), 0)
+        seq_len = tokens * sp_size
+
+        @pl.when(me < sp_size - 1)
+        def _():
+            halo(layer, True).start()
+
+        @pl.when(me > 0)
+        def _():
+            halo(layer, False).start()
+
+        @pl.when(me == 0)
+        def _():
+            uhalo[layer, pl.ds(0, edge), :] = jnp.zeros((edge, half), jnp.bfloat16)
+
+        @pl.when(me == sp_size - 1)
+        def _():
+            uhalo[layer, pl.ds(edge + tokens, edge), :] = jnp.zeros((edge, half), jnp.bfloat16)
+
+        @pl.when(me > 0)
+        def _():
+            halo(layer, True).wait_recv()
+
+        @pl.when(me < sp_size - 1)
+        def _():
+            halo(layer, False).wait_recv()
+
+        for j in range(groups):
+            left = jnp.left_shift(1, t * groups + j)
+            band = jnp.where((col >= row - left) & (col <= row + left - 1), 1.0, 0.0).astype(
+                jnp.bfloat16
+            )
+            cols = slice(j * cg, (j + 1) * cg)
+            wsum = jnp.dot(band, uhalo[layer, :, cols], preferred_element_type=jnp.float32)
+            upper = jnp.minimum(where + left, seq_len)
+            lower = jnp.maximum(where - left, 0)
+            counted = (upper - lower).astype(jnp.float32)
+            pooled = wsum / counted - uhalo[layer, pl.ds(edge, tokens), cols].astype(jnp.float32)
+            mapped = jnp.dot(
+                pooled.astype(jnp.bfloat16), pool_ref[layer, j], preferred_element_type=jnp.float32
+            )
+            mix_send[layer, j] = (mapped * pscale_ref[layer : layer + 1, cols]).astype(jnp.bfloat16)
+            if j > 0:
+                x_copy(1, layer, j - 1).start()
+        return lambda: x_copy(1, layer, groups - 1).start()
+
+    step = cg
+
+    def outward_own(layer):
+        for n in range(0, width_here, step):
+            total = None
+            for j in range(groups):
+                start = pl.multiple_of(t * half + j * cg, cg)
+                block = weights[2 * layer + 1, pl.ds(start, cg), n : n + step]
+                term = jnp.dot(mix_send[layer, j], block, preferred_element_type=jnp.float32)
+                total = term if total is None else total + term
+            acc[:, n : n + step] = total + xcur[:, n : n + step].astype(jnp.float32)
+
+    def outward_peer(layer):
+        squares = jnp.zeros((tokens, 1), jnp.float32)
+        for j in range(groups):
+            x_copy(1, layer, j).wait_recv()
+        for n in range(0, width_here, step):
+            total = acc[:, n : n + step]
+            for j in range(groups):
+                start = pl.multiple_of(peer * half + j * cg, cg)
+                block = weights[2 * layer + 1, pl.ds(start, cg), n : n + step]
+                total = total + jnp.dot(
+                    mix_recv[layer, j], block, preferred_element_type=jnp.float32
+                )
+            stored = total.astype(jnp.bfloat16)
+            xcur[:, n : n + step] = stored
+            value = stored.astype(jnp.float32)
+            squares = squares + jnp.sum(value * value, axis=1, keepdims=True)
+            if layer + 1 < LAYERS:
+                xg[:, n : n + step] = (
+                    value * gain_ref[layer + 1 : layer + 2, n : n + step]
+                ).astype(jnp.bfloat16)
+        store_squares(layer + 1, squares)
+
+    each_own(0, begin)
+    squares = jnp.zeros((tokens, 1), jnp.float32)
+    for n in range(0, width_here, step):
+        value = resid_ref[:, n : n + step].astype(jnp.float32)
+        squares = squares + jnp.sum(value * value, axis=1, keepdims=True)
+        xcur[:, n : n + step] = resid_ref[:, n : n + step]
+        xg[:, n : n + step] = (value * gain_ref[0:1, n : n + step]).astype(jnp.bfloat16)
+    store_squares(0, squares)
+    for stage in range(2 * LAYERS):
+        weights[stage, pl.ds(pl.multiple_of(me * rows, rows), rows), :] = own_w[stage]
+    send_squares(0).start()
+
+    process(0)
+    settle(0)
+    for layer in range(LAYERS):
+        inward(layer)
+        process(2 * layer + 1)
+        last = pooling(layer)
+        last()
+        settle(2 * layer + 1)
+        outward_own(layer)
+        if layer + 1 < LAYERS:
+            process(2 * layer + 2)
+        outward_peer(layer)
+        if layer + 1 < LAYERS:
+            settle(2 * layer + 2)
+        send_squares(layer + 1).start()
+    for stage in range(2 * LAYERS):
+        finish(stage)
+    for kind in range(2):
+        for layer in range(LAYERS):
+            for j in range(groups):
+                x_copy(kind, layer, j).wait_send()
+    for layer in range(LAYERS):
+
+        @pl.when(me < sp_size - 1)
+        def _(layer=layer):
+            halo(layer, True).wait_send()
+
+        @pl.when(me > 0)
+        def _(layer=layer):
+            halo(layer, False).wait_send()
+
+    factor = norm_factor(LAYERS)
+    for n in range(0, width_here, step):
+        out_ref[:, n : n + step] = (
+            xcur[:, n : n + step].astype(jnp.float32) * factor * final_ref[0:1, n : n + step]
+        ).astype(jnp.bfloat16)
+    for k in range(LAYERS + 1):
+        send_squares(k).wait_send()
+
+
+def one_kernel(resid, norm_gain, w_in, w_pool, pool_scale, w_out, final_gain):
+    sp_size = lax.axis_size("sp")
+    depth = sp_size // 4
+    tokens, width_here = resid.shape
+    rows = w_out.shape[1]
+    groups, cg = w_pool.shape[1], w_pool.shape[2]
+    half = groups * cg
+    edge = 2 * margin
+    turned = jnp.swapaxes(w_in, 1, 2)
+    pieces = jnp.stack([turned, w_out], axis=1).reshape(2 * LAYERS, rows, width_here)
+    vmem = pl.BlockSpec(memory_space=pltpu.VMEM)
+    bf, f32 = jnp.bfloat16, jnp.float32
+    dma = pltpu.SemaphoreType.DMA
+    crossing = pltpu.VMEM((LAYERS, groups, tokens, cg), bf)
+    return pl.pallas_call(
+        functools.partial(fused, sp_size),
+        out_shape=jax.ShapeDtypeStruct(resid.shape, bf),
+        in_specs=[vmem] * 6,
+        out_specs=vmem,
+        scratch_shapes=[
+            pltpu.VMEM((2 * LAYERS, sp_size * rows, width_here), bf),
+            pltpu.VMEM((tokens, width_here), bf),
+            pltpu.VMEM((tokens, width_here), bf),
+            pltpu.VMEM((tokens, half), f32),
+            pltpu.VMEM((tokens, width_here), f32),
+            crossing,
+            crossing,
+            pltpu.VMEM((LAYERS, tokens + 2 * edge, half), bf),
+            crossing,
+            crossing,
+            pltpu.VMEM((LAYERS + 1, 8, tokens), f32),
+            pltpu.VMEM((LAYERS + 1, 8, tokens), f32),
+            dma((2 * LAYERS, 5 * depth)),
+            dma((2 * LAYERS, sp_size)),
+            dma((2 * LAYERS * groups,)),
+            dma((2 * LAYERS * groups,)),
+            dma((2 * LAYERS,)),
+            dma((2 * LAYERS,)),
+            dma((LAYERS + 1,)),
+            dma((LAYERS + 1,)),
+        ],
+        compiler_params=pltpu.CompilerParams(
+            collective_id=0, has_side_effects=True, vmem_limit_bytes=48 * 2**20
+        ),
+    )(resid, norm_gain, final_gain[None, :], pieces, w_pool, pool_scale)
+
+
+def spread(*args):
+    resid, w_pool, w_out = args[0], args[3], args[5]
+    fits = (
+        lax.axis_size("tp") == 2
+        and lax.axis_size("sp") % 4 == 0
+        and w_out.shape[1] % 16 == 0
+        and resid.shape[0] % 128 == 0
+        and w_pool.shape[2] % 128 == 0
+        and resid.shape[1] % w_pool.shape[2] == 0
+    )
+    return one_kernel(*args) if fits else shards(*args)
+
+
 def solution(mesh):
     placed = (
         P("sp", "tp"),
@@ -114,5 +572,5 @@
         P("tp"),
     )
     return jax.shard_map(
-        shards, mesh=mesh, in_specs=placed, out_specs=P("sp", "tp"), check_vma=False
-    )
+        spread, mesh=mesh, in_specs=placed, out_specs=P("sp", "tp"), check_vma=False
+    )

time: 190 us -> 83.5 us (0.44)
  waiting for transfers between devices: 115 us -> 0 us
  Pallas kernels: 0 us -> 80.2 us
  blocking collectives: 32.6 us -> 0 us
  between operations: 13.3 us -> 0.06 us
  matrix products: 10.1 us -> 0 us
  other arithmetic: 9.01 us -> 1.12 us
  starting transfers between devices: 5.85 us -> 0 us
    all_gather x2 -> x0, waiting for transfers between devices: 81.5 us -> none  [the longest x1 47.5 us: shards(): lax.all_gather(w_in, 'sp', axis=2, tiled=True)]
    pallas_call x0 -> x1, Pallas kernels: none -> 80.2 us  [one_kernel(): pl.pallas_call(functools.partial(fused, sp_size), out_shape=jax.ShapeDtyp...]
    reduce_scatter x2 -> x0, waiting for transfers between devices: 25.8 us -> none  [shards(): lax.psum_scatter(partial_value, 'tp', scatter_dimension=1, tiled=True)]
    all_gather x2 -> x0, blocking collectives: 16.8 us -> none  [shards(): mixed_all = lax.all_gather(mixed, 'tp', axis=1, tiled=True)]
    psum x3 -> x0, blocking collectives: 15.7 us -> none  [scaled(): squares = lax.psum(jnp.sum(xf * xf, axis=1), 'tp')]
    dot_general x6 -> x0, matrix products: 10.1 us -> none  [the longest x2 6.48 us: shards(): jnp.dot(own_hidden, in_block, preferred_element_type=jnp.float32)]
    convert_element_type x9 -> x0, other arithmetic: 7.38 us -> none  [the longest x2 4.09 us: shards(): pooled = (wsum / counted - upward.astype(jnp.float32)).astype(jnp.bfloat16)]
    ppermute x4 -> x0, waiting for transfers between devices: 6.35 us -> none  [the longest x2 6.35 us: padded_2(): after = lax.ppermute(initial, axis, down)]
  transfers between devices with their start and end apart: 8 -> 0, of which waited for: 6 -> 0; matrix products, arithmetic and copies ran while one was open for 3% -> 0% of each run, Pallas kernels for 0% -> 0%
where the time goes in v1:
time: 83.5 us; the launch traced here: 83.3 us
  Pallas kernels  80.2 us (96%)
  local copies, waits for them, and re-layouts  1.96 us (2%)
  other arithmetic  1.12 us (1%)
    pallas_call x1, Pallas kernels, one_kernel(): pl.pallas_call(functools.partial(fused, sp_size), out_shape=jax.ShapeDtyp...  80.2 us
    unnamed x11, local copies, waits for them, and re-layouts  1.92 us

profile of v1, /device:TPU:0, one launch (start us, length us, event | category | flops | bytes accessed | tf_op | source)
XLA Modules:
  0.0 83.3 jit_solution(6484425977849994819)
XLA Ops:
  0.0 0.0 copy-start.2
  0.0 0.0 copy-start.3
  0.0 0.0 copy-start.4
  0.0 1.1 %pad_maximum_fusion = bf16[2,2,64,1024]{3,2,0,1:T(8,128)(2,1)S(1)} fusion(bf16[2,1,64,1024]{3,2,0,1:T(8,128)(2,1)} %bitcast.8, bf16[2,1,64,1024]{3,2,0,1:T(8,128)(2,1)} %bitcast.9), kind=kLoop, calls=%fused_computation | loop fusion | flops 262144 | bytes 1048576 | tf_op jit(solution)/shard_map/stack | solution.py:513
  1.1 0.0 copy-start
  1.1 0.0 copy-start.1
  1.2 0.0 copy-done.2
  1.2 0.0 copy-done.3
  1.2 0.0 copy-done.4
  1.2 0.9 %copy-done = bf16[256,1024]{1,0:T(8,128)(2,1)S(1)} copy-done((bf16[256,1024]{1,0:T(8,128)(2,1)S(1)}, bf16[256,1024]{1,0:T(8,128)(2,1)}, u32[]{:S(2)}) %copy-start) | copy-done | bytes 524312
  2.2 0.2 copy-done.1
  2.3 80.2 %shard_map.73 = bf16[256,1024]{1,0:T(8,128)(2,1)S(1)} custom-call(bf16[256,1024]{1,0:T(8,128)(2,1)S(1)} %copy-done, f32[2,1024]{1,0:T(2,128)S(1)} %copy-done.2, f32[1,1024]{1,0:T(1,128)S(1)} %bitcast.7, bf16[4,64,1024]{2,1,0:T(8,128)(2,1)S(1)} %bitcast.6, bf16[2,2,256,256]{3,2,1,0:T(8,128)(2,1)S(1)} %copy-done.1, f32[2,512]{1,0:T(2,128)S(1)} %copy-done.4), custom_call_target="tpu_custom_call" | custom-call | tf_op jit(solution)/shard_map/pallas_call | solution.py:518
  82.5 0.8 copy.10
  (1 shorter events, 0.0 us)
Async XLA Ops:
  0.0 1.2 %copy-start.2 = (f32[2,1024]{1,0:T(2,128)S(1)}, f32[2,1024]{1,0:T(2,128)}, u32[]{:S(2)}) copy-start(f32[2,1024]{1,0:T(2,128)} %gain_ref.1) | copy-start | bytes 24580
  0.0 1.2 %copy-start.3 = (f32[1024]{0:T(1024)S(1)}, f32[1024]{0:T(1024)}, u32[]{:S(2)}) copy-start(f32[1024]{0:T(1024)} %param.13) | copy-start | bytes 12292
  0.0 1.2 %copy-start.4 = (f32[2,512]{1,0:T(2,128)S(1)}, f32[2,512]{1,0:T(2,128)}, u32[]{:S(2)}) copy-start(f32[2,512]{1,0:T(2,128)} %pscale_ref.1) | copy-start | bytes 12292
  1.1 1.0 %copy-start = (bf16[256,1024]{1,0:T(8,128)(2,1)S(1)}, bf16[256,1024]{1,0:T(8,128)(2,1)}, u32[]{:S(2)}) copy-start(bf16[256,1024]{1,0:T(8,128)(2,1)} %resid_ref.1) | copy-start | bytes 1572868
  1.1 1.2 %copy-start.1 = (bf16[2,2,256,256]{3,2,1,0:T(8,128)(2,1)S(1)}, bf16[2,2,256,256]{3,2,1,0:T(8,128)(2,1)}, u32[]{:S(2)}) copy-start(bf16[2,2,256,256]{3,2,1,0:T(8,128)(2,1)} %pool_ref.1) | copy-start | bytes 1572868

commit v2 on v1

--- a/solution.py
+++ b/solution.py
@@ -171,6 +171,8 @@
     for ok, who in (
         (z > 0, me - 4),
         (z < depth - 1, me + 4),
+        (z > 1, me - 8),
+        (z < depth - 2, me + 8),
         (me > 0, me - 1),
         (me < sp_size - 1, me + 1),
     ):
@@ -183,6 +185,8 @@
         3
         + jnp.where(z > 0, 1, 0)
         + jnp.where(z < depth - 1, 1, 0)
+        + jnp.where(z > 1, 1, 0)
+        + jnp.where(z < depth - 2, 1, 0)
         + jnp.where(me > 0, 1, 0)
         + jnp.where(me < sp_size - 1, 1, 0)
     )
@@ -193,7 +197,15 @@
 
     def hop(stage, zz, yy, way, target, from_own=False):
         piece = number(zz, yy, core)
-        slot = {"sib": zz * 2 + yy, "y": 2 * depth + zz, "up": 3 * depth + zz, "down": 4 * depth + zz}[way]
+        slot = {
+            "sib": zz * 2 + yy,
+            "y": 2 * depth + zz,
+            "up1": 3 * depth + zz,
+            "down1": 4 * depth + zz,
+            "up2": 5 * depth,
+            "down2": 5 * depth + 1,
+            "pair": 5 * depth + 2,
+        }[way]
         return pltpu.make_async_remote_copy(
             src_ref=own_w.at[stage] if from_own else landing(stage, piece),
             dst_ref=landing(stage, piece),
@@ -215,40 +227,63 @@
         ).wait_recv()
 
     def each_own(stage, act):
-        @pl.when(z < depth - 1)
-        def _():
-            act(hop(stage, z, y, "up", me + 4, True))
-
-        @pl.when(z > 0)
-        def _():
-            act(hop(stage, z, y, "down", me - 4, True))
-
+        for d in (2, 1):
+
+            @pl.when(z + d < depth)
+            def _(d=d):
+                act(hop(stage, z, y, f"up{d}", me + 4 * d, True))
+
+            @pl.when(z - d >= 0)
+            def _(d=d):
+                act(hop(stage, z, y, f"down{d}", me - 4 * d, True))
+
+        act(hop(stage, z, y, "sib", sibling, True))
+
+    def own_y(stage, act):
         act(hop(stage, z, y, "y", across, True))
-        act(hop(stage, z, y, "sib", sibling, True))
+
+    zpair = z + 1 - 2 * lax.rem(z, 2)
+    by_pair = (core == 1) & (zpair < depth)
 
     def each_z(stage, d, act, arrive):
         @pl.when(z - d >= 0)
         def _():
             if arrive:
                 wait_piece(stage, z - d, y, core)
-
-            @pl.when(z < depth - 1)
-            def _():
-                act(hop(stage, z - d, y, "up", me + 4))
-
-            act(hop(stage, z - d, y, "y", across))
+            if d >= 2:
+
+                @pl.when(z < depth - 1)
+                def _():
+                    act(hop(stage, z - d, y, "up1", me + 4))
+
+            if d > 1:
+                act(hop(stage, z - d, y, "y", across))
+            else:
+
+                @pl.when(jnp.logical_not(by_pair & (zpair == z - 1)))
+                def _():
+                    act(hop(stage, z - 1, y, "y", across))
+
             act(hop(stage, z - d, y, "sib", sibling))
 
         @pl.when(z + d < depth)
         def _():
             if arrive:
                 wait_piece(stage, z + d, y, core)
-
-            @pl.when(z > 0)
-            def _():
-                act(hop(stage, z + d, y, "down", me - 4))
-
-            act(hop(stage, z + d, y, "y", across))
+            if d >= 2:
+
+                @pl.when(z > 0)
+                def _():
+                    act(hop(stage, z + d, y, "down1", me - 4))
+
+            if d > 1:
+                act(hop(stage, z + d, y, "y", across))
+            else:
+
+                @pl.when(jnp.logical_not(by_pair & (zpair == z + 1)))
+                def _():
+                    act(hop(stage, z + 1, y, "y", across))
+
             act(hop(stage, z + d, y, "sib", sibling))
 
     def each_y(stage, d, act, arrive):
@@ -259,6 +294,11 @@
 
         if d == 0:
             one(z)
+
+            @pl.when(by_pair)
+            def _():
+                act(hop(stage, z, 1 - y, "pair", number(zpair, y, core)))
+
         else:
 
             @pl.when(z - d >= 0)
@@ -272,13 +312,35 @@
     begin = lambda copy: copy.start()
     drain = lambda copy: copy.wait_send()
 
-    def process(stage):
-        for d in range(1, depth):
+    def step_own(stage):
+        if stage < 2 * LAYERS:
+            each_own(stage, begin)
+        if stage + 1 < 2 * LAYERS:
+            own_y(stage + 1, begin)
+
+    def step_z(stage, d):
+        if stage < 2 * LAYERS and d < depth:
             each_z(stage, d, begin, True)
-            if d == depth - 1 and stage + 1 < 2 * LAYERS:
-                each_own(stage + 1, begin)
-            each_y(stage, d - 1, begin, True)
-        each_y(stage, depth - 1, begin, True)
+
+    def step_y(stage, d):
+        if stage < 2 * LAYERS and d < depth:
+            each_y(stage, d, begin, True)
+
+    def opening(stage):
+        step_y(stage, 0)
+        step_z(stage, 2)
+        step_own(stage + 2)
+        step_y(stage, 1)
+
+    def closing(stage, ahead=True):
+        for d in range(3, depth):
+            step_z(stage, d)
+        if ahead:
+            step_z(stage + 1, 1)
+        for d in range(2, depth):
+            step_y(stage, d)
+        if not ahead:
+            step_z(stage + 1, 1)
 
     def settle(stage):
         for zz in range(depth):
@@ -287,6 +349,7 @@
 
     def finish(stage):
         each_own(stage, drain)
+        own_y(stage, drain)
         for d in range(1, depth):
             each_z(stage, d, drain, False)
         for d in range(depth):
@@ -328,14 +391,14 @@
             device_id_type=MESH,
         )
 
-    def halo(layer, upward):
+    def halo(layer, j, upward):
         if upward:
-            source = uhalo.at[layer, pl.ds(tokens, edge), :]
-            target = uhalo.at[layer, pl.ds(0, edge), :]
+            source = uhalo.at[layer, j, pl.ds(tokens, edge), :]
+            target = uhalo.at[layer, j, pl.ds(0, edge), :]
         else:
-            source = uhalo.at[layer, pl.ds(edge, edge), :]
-            target = uhalo.at[layer, pl.ds(edge + tokens, edge), :]
-        k = layer * 2 + (1 if upward else 0)
+            source = uhalo.at[layer, j, pl.ds(edge, edge), :]
+            target = uhalo.at[layer, j, pl.ds(edge + tokens, edge), :]
+        k = (layer * groups + j) * 2 + (1 if upward else 0)
         return pltpu.make_async_remote_copy(
             src_ref=source,
             dst_ref=target,
@@ -345,6 +408,15 @@
             device_id_type=MESH,
         )
 
+    def each_halo(layer, j, act):
+        @pl.when(me < sp_size - 1)
+        def _():
+            act(halo(layer, j, True))
+
+        @pl.when(me > 0)
+        def _():
+            act(halo(layer, j, False))
+
     def project(layer, which, j):
         start = pl.multiple_of(which * half + j * cg, cg)
         block = weights[2 * layer, pl.ds(start, cg), :]
@@ -364,56 +436,37 @@
         for j in range(groups):
             x_copy(0, layer, j).wait_recv()
             value = own_part[:, j * cg : (j + 1) * cg] + part_recv[layer, j].astype(jnp.float32)
-            uhalo[layer, pl.ds(edge, tokens), j * cg : (j + 1) * cg] = (value * factor).astype(
-                jnp.bfloat16
-            )
+            uhalo[layer, j, pl.ds(edge, tokens), :] = (value * factor).astype(jnp.bfloat16)
+            each_halo(layer, j, begin)
         row = lax.broadcasted_iota(jnp.int32, (tokens, tokens + 2 * edge), 0)
         col = lax.broadcasted_iota(jnp.int32, (tokens, tokens + 2 * edge), 1) - edge
         where = me * tokens + lax.broadcasted_iota(jnp.int32, (tokens, 1), 0)
         seq_len = tokens * sp_size
-
-        @pl.when(me < sp_size - 1)
-        def _():
-            halo(layer, True).start()
-
-        @pl.when(me > 0)
-        def _():
-            halo(layer, False).start()
-
-        @pl.when(me == 0)
-        def _():
-            uhalo[layer, pl.ds(0, edge), :] = jnp.zeros((edge, half), jnp.bfloat16)
-
-        @pl.when(me == sp_size - 1)
-        def _():
-            uhalo[layer, pl.ds(edge + tokens, edge), :] = jnp.zeros((edge, half), jnp.bfloat16)
-
-        @pl.when(me > 0)
-        def _():
-            halo(layer, True).wait_recv()
-
-        @pl.when(me < sp_size - 1)
-        def _():
-            halo(layer, False).wait_recv()
-
         for j in range(groups):
             left = jnp.left_shift(1, t * groups + j)
             band = jnp.where((col >= row - left) & (col <= row + left - 1), 1.0, 0.0).astype(
                 jnp.bfloat16
             )
-            cols = slice(j * cg, (j + 1) * cg)
-            wsum = jnp.dot(band, uhalo[layer, :, cols], preferred_element_type=jnp.float32)
             upper = jnp.minimum(where + left, seq_len)
             lower = jnp.maximum(where - left, 0)
-            counted = (upper - lower).astype(jnp.float32)
-            pooled = wsum / counted - uhalo[layer, pl.ds(edge, tokens), cols].astype(jnp.float32)
+            inverse = 1.0 / (upper - lower).astype(jnp.float32)
+
+            @pl.when(me > 0)
+            def _(j=j):
+                halo(layer, j, True).wait_recv()
+
+            @pl.when(me < sp_size - 1)
+            def _(j=j):
+                halo(layer, j, False).wait_recv()
+
+            wsum = jnp.dot(band, uhalo[layer, j], preferred_element_type=jnp.float32)
+            pooled = wsum * inverse - uhalo[layer, j, pl.ds(edge, tokens), :].astype(jnp.float32)
             mapped = jnp.dot(
                 pooled.astype(jnp.bfloat16), pool_ref[layer, j], preferred_element_type=jnp.float32
             )
-            mix_send[layer, j] = (mapped * pscale_ref[layer : layer + 1, cols]).astype(jnp.bfloat16)
-            if j > 0:
-                x_copy(1, layer, j - 1).start()
-        return lambda: x_copy(1, layer, groups - 1).start()
+            scale = pscale_ref[layer : layer + 1, j * cg : (j + 1) * cg]
+            mix_send[layer, j] = (mapped * scale).astype(jnp.bfloat16)
+            x_copy(1, layer, j).start()
 
     step = cg
 
@@ -449,7 +502,9 @@
                 ).astype(jnp.bfloat16)
         store_squares(layer + 1, squares)
 
-    each_own(0, begin)
+    own_y(0, begin)
+    step_own(0)
+    step_own(1)
     squares = jnp.zeros((tokens, 1), jnp.float32)
     for n in range(0, width_here, step):
         value = resid_ref[:, n : n + step].astype(jnp.float32)
@@ -457,25 +512,38 @@
         xcur[:, n : n + step] = resid_ref[:, n : n + step]
         xg[:, n : n + step] = (value * gain_ref[0:1, n : n + step]).astype(jnp.bfloat16)
     store_squares(0, squares)
+    nothing = jnp.zeros((LAYERS, groups, edge, cg), jnp.bfloat16)
+
+    @pl.when(me == 0)
+    def _():
+        uhalo[:, :, pl.ds(0, edge), :] = nothing
+
+    @pl.when(me == sp_size - 1)
+    def _():
+        uhalo[:, :, pl.ds(edge + tokens, edge), :] = nothing
+
     for stage in range(2 * LAYERS):
         weights[stage, pl.ds(pl.multiple_of(me * rows, rows), rows), :] = own_w[stage]
     send_squares(0).start()
 
-    process(0)
+    step_z(0, 1)
+    opening(0)
+    closing(0, False)
     settle(0)
     for layer in range(LAYERS):
         inward(layer)
-        process(2 * layer + 1)
-        last = pooling(layer)
-        last()
+        opening(2 * layer + 1)
+        pooling(layer)
+        closing(2 * layer + 1)
         settle(2 * layer + 1)
         outward_own(layer)
         if layer + 1 < LAYERS:
-            process(2 * layer + 2)
+            opening(2 * layer + 2)
         outward_peer(layer)
+        send_squares(layer + 1).start()
         if layer + 1 < LAYERS:
+            closing(2 * layer + 2)
             settle(2 * layer + 2)
-        send_squares(layer + 1).start()
     for stage in range(2 * LAYERS):
         finish(stage)
     for kind in range(2):
@@ -483,14 +551,8 @@
             for j in range(groups):
                 x_copy(kind, layer, j).wait_send()
     for layer in range(LAYERS):
-
-        @pl.when(me < sp_size - 1)
-        def _(layer=layer):
-            halo(layer, True).wait_send()
-
-        @pl.when(me > 0)
-        def _(layer=layer):
-            halo(layer, False).wait_send()
+        for j in range(groups):
+            each_halo(layer, j, drain)
 
     factor = norm_factor(LAYERS)
     for n in range(0, width_here, step):
@@ -528,17 +590,17 @@
             pltpu.VMEM((tokens, width_here), f32),
             crossing,
             crossing,
-            pltpu.VMEM((LAYERS, tokens + 2 * edge, half), bf),
+            pltpu.VMEM((LAYERS, groups, tokens + 2 * edge, cg), bf),
             crossing,
             crossing,
             pltpu.VMEM((LAYERS + 1, 8, tokens), f32),
             pltpu.VMEM((LAYERS + 1, 8, tokens), f32),
-            dma((2 * LAYERS, 5 * depth)),
+            dma((2 * LAYERS, 5 * depth + 3)),
             dma((2 * LAYERS, sp_size)),
             dma((2 * LAYERS * groups,)),
             dma((2 * LAYERS * groups,)),
-            dma((2 * LAYERS,)),
-            dma((2 * LAYERS,)),
+            dma((2 * LAYERS * groups,)),
+            dma((2 * LAYERS * groups,)),
             dma((LAYERS + 1,)),
             dma((LAYERS + 1,)),
         ],

time: 83.5 us -> 78.6 us (0.941)
  Pallas kernels: 80.2 us -> 75.3 us
    pallas_call x1, Pallas kernels: 80.2 us -> 75.3 us  [one_kernel(): pl.pallas_call(functools.partial(fused, sp_size), out_shape=jax.ShapeDtyp...]
where the time goes in v2:
time: 78.6 us; the launch traced here: 78.5 us
  Pallas kernels  75.3 us (96%)
  local copies, waits for them, and re-layouts  1.96 us (2%)
  other arithmetic  1.12 us (1%)
    pallas_call x1, Pallas kernels, one_kernel(): pl.pallas_call(functools.partial(fused, sp_size), out_shape=jax.ShapeDtyp...  75.3 us
    unnamed x11, local copies, waits for them, and re-layouts  1.92 us

profile of v2, /device:TPU:0, one launch (start us, length us, event | category | flops | bytes accessed | tf_op | source)
XLA Modules:
  0.0 78.5 jit_solution(16240446894486863461)
XLA Ops:
  0.0 0.0 copy-start.2
  0.0 0.0 copy-start.3
  0.0 0.0 copy-start.4
  0.0 1.1 %pad_maximum_fusion = bf16[2,2,64,1024]{3,2,0,1:T(8,128)(2,1)S(1)} fusion(bf16[2,1,64,1024]{3,2,0,1:T(8,128)(2,1)} %bitcast.8, bf16[2,1,64,1024]{3,2,0,1:T(8,128)(2,1)} %bitcast.9), kind=kLoop, calls=%fused_computation | loop fusion | flops 262144 | bytes 1048576 | tf_op jit(solution)/shard_map/stack | solution.py:575
  1.1 0.0 copy-start
  1.1 0.0 copy-start.1
  1.2 0.0 copy-done.2
  1.2 0.0 copy-done.3
  1.2 0.0 copy-done.4
  1.2 0.9 %copy-done = bf16[256,1024]{1,0:T(8,128)(2,1)S(1)} copy-done((bf16[256,1024]{1,0:T(8,128)(2,1)S(1)}, bf16[256,1024]{1,0:T(8,128)(2,1)}, u32[]{:S(2)}) %copy-start) | copy-done | bytes 524312
  2.2 0.2 copy-done.1
  2.3 75.3 %shard_map.73 = bf16[256,1024]{1,0:T(8,128)(2,1)S(1)} custom-call(bf16[256,1024]{1,0:T(8,128)(2,1)S(1)} %copy-done, f32[2,1024]{1,0:T(2,128)S(1)} %copy-done.2, f32[1,1024]{1,0:T(1,128)S(1)} %bitcast.7, bf16[4,64,1024]{2,1,0:T(8,128)(2,1)S(1)} %bitcast.6, bf16[2,2,256,256]{3,2,1,0:T(8,128)(2,1)S(1)} %copy-done.1, f32[2,512]{1,0:T(2,128)S(1)} %copy-done.4), custom_call_target="tpu_custom_call" | custom-call | tf_op jit(solution)/shard_map/pallas_call | solution.py:580
  77.7 0.8 %copy.10 = bf16[256,1024]{1,0:T(8,128)(2,1)} copy(bf16[256,1024]{1,0:T(8,128)(2,1)S(1)} %shard_map.73) | data formatting | bytes 1048576
  (1 shorter events, 0.0 us)
Async XLA Ops:
  0.0 1.2 %copy-start.2 = (f32[2,1024]{1,0:T(2,128)S(1)}, f32[2,1024]{1,0:T(2,128)}, u32[]{:S(2)}) copy-start(f32[2,1024]{1,0:T(2,128)} %gain_ref.1) | copy-start | bytes 24580
  0.0 1.2 %copy-start.3 = (f32[1024]{0:T(1024)S(1)}, f32[1024]{0:T(1024)}, u32[]{:S(2)}) copy-start(f32[1024]{0:T(1024)} %param.13) | copy-start | bytes 12292
  0.0 1.2 %copy-start.4 = (f32[2,512]{1,0:T(2,128)S(1)}, f32[2,512]{1,0:T(2,128)}, u32[]{:S(2)}) copy-start(f32[2,512]{1,0:T(2,128)} %pscale_ref.1) | copy-start | bytes 12292
  1.1 1.0 %copy-start = (bf16[256,1024]{1,0:T(8,128)(2,1)S(1)}, bf16[256,1024]{1,0:T(8,128)(2,1)}, u32[]{:S(2)}) copy-start(bf16[256,1024]{1,0:T(8,128)(2,1)} %resid_ref.1) | copy-start | bytes 1572868
  1.1 1.2 %copy-start.1 = (bf16[2,2,256,256]{3,2,1,0:T(8,128)(2,1)S(1)}, bf16[2,2,256,256]{3,2,1,0:T(8,128)(2,1)}, u32[]{:S(2)}) copy-start(bf16[2,2,256,256]{3,2,1,0:T(8,128)(2,1)} %pool_ref.1) | copy-start | bytes 1572868

commit v3 on v2

--- a/solution.py
+++ b/solution.py
@@ -122,13 +122,12 @@
     weights,
     xg,
     xcur,
-    own_part,
-    acc,
     part_send,
     part_recv,
     uhalo,
-    mix_send,
-    mix_recv,
+    mixed,
+    pool_all,
+    pscale_all,
     ss_send,
     ss_recv,
     w_send_sem,
@@ -139,12 +138,14 @@
     h_recv_sem,
     s_send_sem,
     s_recv_sem,
+    p_send_sem,
+    p_recv_sem,
 ):
     depth = sp_size // 4
     rows = own_w.shape[1]
     tokens, width_here = resid_ref.shape
     groups, cg = pool_ref.shape[1], pool_ref.shape[2]
-    half = groups * cg
+    total_groups = 2 * groups
     width = 2 * width_here
     edge = 2 * margin
     me = lax.axis_index("sp")
@@ -227,7 +228,7 @@
         ).wait_recv()
 
     def each_own(stage, act):
-        for d in (2, 1):
+        for d in (1, 2):
 
             @pl.when(z + d < depth)
             def _(d=d):
@@ -379,14 +380,23 @@
         column = jnp.sum(jnp.where(diagonal, line, 0.0), axis=1, keepdims=True)
         return lax.rsqrt(column / width + eps)
 
-    def x_copy(kind, layer, j):
-        k = (kind * LAYERS + layer) * groups + j
-        source, target = ((part_send, part_recv), (mix_send, mix_recv))[kind]
+    def x_copy(layer, j):
+        k = layer * total_groups + j
         return pltpu.make_async_remote_copy(
-            src_ref=source.at[layer, j],
-            dst_ref=target.at[layer, j],
+            src_ref=part_send.at[layer, j],
+            dst_ref=part_recv.at[layer, j],
             send_sem=x_send_sem.at[k],
             recv_sem=x_recv_sem.at[k],
+            device_id={"tp": peer},
+            device_id_type=MESH,
+        )
+
+    def pool_copy(layer):
+        return pltpu.make_async_remote_copy(
+            src_ref=pool_ref.at[layer] if layer < LAYERS else pscale_ref,
+            dst_ref=pool_all.at[layer, t] if layer < LAYERS else pscale_all.at[t],
+            send_sem=p_send_sem.at[layer],
+            recv_sem=p_recv_sem.at[layer],
             device_id={"tp": peer},
             device_id_type=MESH,
         )
@@ -398,7 +408,7 @@
         else:
             source = uhalo.at[layer, j, pl.ds(edge, edge), :]
             target = uhalo.at[layer, j, pl.ds(edge + tokens, edge), :]
-        k = (layer * groups + j) * 2 + (1 if upward else 0)
+        k = (layer * total_groups + j) * 2 + (1 if upward else 0)
         return pltpu.make_async_remote_copy(
             src_ref=source,
             dst_ref=target,
@@ -417,33 +427,59 @@
         def _():
             act(halo(layer, j, False))
 
-    def project(layer, which, j):
-        start = pl.multiple_of(which * half + j * cg, cg)
-        block = weights[2 * layer, pl.ds(start, cg), :]
-        return lax.dot_general(
-            xg[...], block, (((1,), (1,)), ((), ())), preferred_element_type=jnp.float32
-        )
-
-    def inward(layer):
-        for j in range(groups):
-            part_send[layer, j] = project(layer, peer, j).astype(jnp.bfloat16)
-        for j in range(groups):
-            x_copy(0, layer, j).start()
-            own_part[:, j * cg : (j + 1) * cg] = project(layer, t, j)
+    def inward(layer, d):
+        def plane(zz):
+            for yy in range(2):
+                wait_piece(2 * layer, zz, yy, 1 - core)
+            block = weights[2 * layer, pl.ds(pl.multiple_of(zz * cg, cg), cg), :]
+            part = lax.dot_general(
+                xg[...], block, (((1,), (1,)), ((), ())), preferred_element_type=jnp.float32
+            )
+            part_send[layer, zz] = part.astype(jnp.bfloat16)
+            x_copy(layer, zz).start()
+
+        if d == 0:
+            plane(z)
+        else:
+
+            @pl.when(z - d >= 0)
+            def _():
+                plane(z - d)
+
+            @pl.when(z + d < depth)
+            def _():
+                plane(z + d)
+
+    def closing_inward(layer):
+        stage = 2 * layer
+        inward(layer, 0)
+        for d in range(3, depth):
+            step_z(stage, d)
+        if layer > 0:
+            step_z(stage + 1, 1)
+        inward(layer, 1)
+        for d in range(2, depth):
+            step_y(stage, d)
+            inward(layer, d)
+        if layer == 0:
+            step_z(stage + 1, 1)
 
     def pooling(layer):
         factor = norm_factor(layer)
-        for j in range(groups):
-            x_copy(0, layer, j).wait_recv()
-            value = own_part[:, j * cg : (j + 1) * cg] + part_recv[layer, j].astype(jnp.float32)
+        pool_copy(layer).wait_recv()
+        if layer == 0:
+            pool_copy(LAYERS).wait_recv()
+        for j in range(total_groups):
+            x_copy(layer, j).wait_recv()
+            value = part_send[layer, j].astype(jnp.float32) + part_recv[layer, j].astype(jnp.float32)
             uhalo[layer, j, pl.ds(edge, tokens), :] = (value * factor).astype(jnp.bfloat16)
             each_halo(layer, j, begin)
         row = lax.broadcasted_iota(jnp.int32, (tokens, tokens + 2 * edge), 0)
         col = lax.broadcasted_iota(jnp.int32, (tokens, tokens + 2 * edge), 1) - edge
         where = me * tokens + lax.broadcasted_iota(jnp.int32, (tokens, 1), 0)
         seq_len = tokens * sp_size
-        for j in range(groups):
-            left = jnp.left_shift(1, t * groups + j)
+        for j in range(total_groups):
+            left = 2**j
             band = jnp.where((col >= row - left) & (col <= row + left - 1), 1.0, 0.0).astype(
                 jnp.bfloat16
             )
@@ -462,36 +498,21 @@
             wsum = jnp.dot(band, uhalo[layer, j], preferred_element_type=jnp.float32)
             pooled = wsum * inverse - uhalo[layer, j, pl.ds(edge, tokens), :].astype(jnp.float32)
             mapped = jnp.dot(
-                pooled.astype(jnp.bfloat16), pool_ref[layer, j], preferred_element_type=jnp.float32
+                pooled.astype(jnp.bfloat16), pool_all[layer, j // groups, j % groups], preferred_element_type=jnp.float32
             )
-            scale = pscale_ref[layer : layer + 1, j * cg : (j + 1) * cg]
-            mix_send[layer, j] = (mapped * scale).astype(jnp.bfloat16)
-            x_copy(1, layer, j).start()
+            first = j % groups * cg
+            scale = pscale_all[j // groups, layer : layer + 1, first : first + cg]
+            mixed[j] = (mapped * scale).astype(jnp.bfloat16)
 
     step = cg
 
-    def outward_own(layer):
+    def outward(layer):
+        squares = jnp.zeros((tokens, 1), jnp.float32)
         for n in range(0, width_here, step):
-            total = None
-            for j in range(groups):
-                start = pl.multiple_of(t * half + j * cg, cg)
-                block = weights[2 * layer + 1, pl.ds(start, cg), n : n + step]
-                term = jnp.dot(mix_send[layer, j], block, preferred_element_type=jnp.float32)
-                total = term if total is None else total + term
-            acc[:, n : n + step] = total + xcur[:, n : n + step].astype(jnp.float32)
-
-    def outward_peer(layer):
-        squares = jnp.zeros((tokens, 1), jnp.float32)
-        for j in range(groups):
-            x_copy(1, layer, j).wait_recv()
-        for n in range(0, width_here, step):
-            total = acc[:, n : n + step]
-            for j in range(groups):
-                start = pl.multiple_of(peer * half + j * cg, cg)
-                block = weights[2 * layer + 1, pl.ds(start, cg), n : n + step]
-                total = total + jnp.dot(
-                    mix_recv[layer, j], block, preferred_element_type=jnp.float32
-                )
+            total = xcur[:, n : n + step].astype(jnp.float32)
+            for j in range(total_groups):
+                block = weights[2 * layer + 1, j * cg : (j + 1) * cg, n : n + step]
+                total = total + jnp.dot(mixed[j], block, preferred_element_type=jnp.float32)
             stored = total.astype(jnp.bfloat16)
             xcur[:, n : n + step] = stored
             value = stored.astype(jnp.float32)
@@ -502,6 +523,8 @@
                 ).astype(jnp.bfloat16)
         store_squares(layer + 1, squares)
 
+    for k in range(LAYERS + 1):
+        pool_copy(k).start()
     own_y(0, begin)
     step_own(0)
     step_own(1)
@@ -512,7 +535,9 @@
         xcur[:, n : n + step] = resid_ref[:, n : n + step]
         xg[:, n : n + step] = (value * gain_ref[0:1, n : n + step]).astype(jnp.bfloat16)
     store_squares(0, squares)
-    nothing = jnp.zeros((LAYERS, groups, edge, cg), jnp.bfloat16)
+    pool_all[:, pl.ds(t, 1)] = pool_ref[...][:, None]
+    pscale_all[pl.ds(t, 1)] = pscale_ref[...][None]
+    nothing = jnp.zeros((LAYERS, total_groups, edge, cg), jnp.bfloat16)
 
     @pl.when(me == 0)
     def _():
@@ -528,30 +553,23 @@
 
     step_z(0, 1)
     opening(0)
-    closing(0, False)
-    settle(0)
     for layer in range(LAYERS):
-        inward(layer)
+        closing_inward(layer)
         opening(2 * layer + 1)
+        closing(2 * layer + 1)
         pooling(layer)
-        closing(2 * layer + 1)
-        settle(2 * layer + 1)
-        outward_own(layer)
         if layer + 1 < LAYERS:
             opening(2 * layer + 2)
-        outward_peer(layer)
+        settle(2 * layer + 1)
+        outward(layer)
         send_squares(layer + 1).start()
-        if layer + 1 < LAYERS:
-            closing(2 * layer + 2)
-            settle(2 * layer + 2)
     for stage in range(2 * LAYERS):
         finish(stage)
-    for kind in range(2):
-        for layer in range(LAYERS):
-            for j in range(groups):
-                x_copy(kind, layer, j).wait_send()
+    for k in range(LAYERS + 1):
+        pool_copy(k).wait_send()
     for layer in range(LAYERS):
-        for j in range(groups):
+        for j in range(total_groups):
+            x_copy(layer, j).wait_send()
             each_halo(layer, j, drain)
 
     factor = norm_factor(LAYERS)
@@ -569,14 +587,13 @@
     tokens, width_here = resid.shape
     rows = w_out.shape[1]
     groups, cg = w_pool.shape[1], w_pool.shape[2]
-    half = groups * cg
     edge = 2 * margin
     turned = jnp.swapaxes(w_in, 1, 2)
     pieces = jnp.stack([turned, w_out], axis=1).reshape(2 * LAYERS, rows, width_here)
     vmem = pl.BlockSpec(memory_space=pltpu.VMEM)
     bf, f32 = jnp.bfloat16, jnp.float32
     dma = pltpu.SemaphoreType.DMA
-    crossing = pltpu.VMEM((LAYERS, groups, tokens, cg), bf)
+    crossing = pltpu.VMEM((LAYERS, 2 * groups, tokens, cg), bf)
     return pl.pallas_call(
         functools.partial(fused, sp_size),
         out_shape=jax.ShapeDtypeStruct(resid.shape, bf),
@@ -586,21 +603,22 @@
             pltpu.VMEM((2 * LAYERS, sp_size * rows, width_here), bf),
             pltpu.VMEM((tokens, width_here), bf),
             pltpu.VMEM((tokens, width_here), bf),
-            pltpu.VMEM((tokens, half), f32),
-            pltpu.VMEM((tokens, width_here), f32),
             crossing,
             crossing,
-            pltpu.VMEM((LAYERS, groups, tokens + 2 * edge, cg), bf),
-            crossing,
-            crossing,
+            pltpu.VMEM((LAYERS, 2 * groups, tokens + 2 * edge, cg), bf),
+            pltpu.VMEM((2 * groups, tokens, cg), bf),
+            pltpu.VMEM((LAYERS, 2, groups, cg, cg), bf),
+            pltpu.VMEM((2, LAYERS, groups * cg), f32),
             pltpu.VMEM((LAYERS + 1, 8, tokens), f32),
             pltpu.VMEM((LAYERS + 1, 8, tokens), f32),
             dma((2 * LAYERS, 5 * depth + 3)),
             dma((2 * LAYERS, sp_size)),
-            dma((2 * LAYERS * groups,)),
-            dma((2 * LAYERS * groups,)),
-            dma((2 * LAYERS * groups,)),
-            dma((2 * LAYERS * groups,)),
+            dma((4 * LAYERS * groups,)),
+            dma((4 * LAYERS * groups,)),
+            dma((4 * LAYERS * groups,)),
+            dma((4 * LAYERS * groups,)),
+            dma((LAYERS + 1,)),
+            dma((LAYERS + 1,)),
             dma((LAYERS + 1,)),
             dma((LAYERS + 1,)),
         ],
@@ -616,6 +634,8 @@
         lax.axis_size("tp") == 2
         and lax.axis_size("sp") % 4 == 0
         and w_out.shape[1] % 16 == 0
+        and 4 * w_out.shape[1] == w_pool.shape[2]
+        and lax.axis_size("sp") // 4 == 2 * w_pool.shape[1]
         and resid.shape[0] % 128 == 0
         and w_pool.shape[2] % 128 == 0
         and resid.shape[1] % w_pool.shape[2] == 0

time: 78.6 us -> 72.8 us (0.926)
  Pallas kernels: 75.3 us -> 69.5 us
    pallas_call x1, Pallas kernels: 75.3 us -> 69.5 us  [one_kernel(): pl.pallas_call(functools.partial(fused, sp_size), out_shape=jax.ShapeDtyp...]
where the time goes in v3:
time: 72.8 us; the launch traced here: 72.6 us
  Pallas kernels  69.5 us (95%)
  local copies, waits for them, and re-layouts  1.96 us (3%)
  other arithmetic  1.12 us (2%)
    pallas_call x1, Pallas kernels, one_kernel(): pl.pallas_call(functools.partial(fused, sp_size), out_shape=jax.ShapeDtyp...  69.5 us
    unnamed x11, local copies, waits for them, and re-layouts  1.92 us

profile of v3, /device:TPU:0, one launch (start us, length us, event | category | flops | bytes accessed | tf_op | source)
XLA Modules:
  0.0 72.6 jit_solution(11574834068752803104)
XLA Ops:
  0.0 0.0 copy-start.2
  0.0 0.0 copy-start.3
  0.0 0.0 copy-start.4
  0.0 1.1 %pad_maximum_fusion = bf16[2,2,64,1024]{3,2,0,1:T(8,128)(2,1)S(1)} fusion(bf16[2,1,64,1024]{3,2,0,1:T(8,128)(2,1)} %bitcast.8, bf16[2,1,64,1024]{3,2,0,1:T(8,128)(2,1)} %bitcast.9), kind=kLoop, calls=%fused_computation | loop fusion | flops 262144 | bytes 1048576 | tf_op jit(solution)/shard_map/stack | solution.py:592
  1.1 0.0 copy-start
  1.1 0.0 copy-start.1
  1.2 0.0 copy-done.2
  1.2 0.0 copy-done.3
  1.2 0.0 copy-done.4
  1.2 0.9 %copy-done = bf16[256,1024]{1,0:T(8,128)(2,1)S(1)} copy-done((bf16[256,1024]{1,0:T(8,128)(2,1)S(1)}, bf16[256,1024]{1,0:T(8,128)(2,1)}, u32[]{:S(2)}) %copy-start) | copy-done | bytes 524312
  2.2 0.2 copy-done.1
  2.3 69.5 %shard_map.73 = bf16[256,1024]{1,0:T(8,128)(2,1)S(1)} custom-call(bf16[256,1024]{1,0:T(8,128)(2,1)S(1)} %copy-done, f32[2,1024]{1,0:T(2,128)S(1)} %copy-done.2, f32[1,1024]{1,0:T(1,128)S(1)} %bitcast.7, bf16[4,64,1024]{2,1,0:T(8,128)(2,1)S(1)} %bitcast.6, bf16[2,2,256,256]{3,2,1,0:T(8,128)(2,1)S(1)} %copy-done.1, f32[2,512]{1,0:T(2,128)S(1)} %copy-done.4), custom_call_target="tpu_custom_call" | custom-call | tf_op jit(solution)/shard_map/pallas_call | solution.py:597
  71.8 0.8 %copy.10 = bf16[256,1024]{1,0:T(8,128)(2,1)} copy(bf16[256,1024]{1,0:T(8,128)(2,1)S(1)} %shard_map.73) | data formatting | bytes 1048576
  (1 shorter events, 0.0 us)
Async XLA Ops:
  0.0 1.2 %copy-start.2 = (f32[2,1024]{1,0:T(2,128)S(1)}, f32[2,1024]{1,0:T(2,128)}, u32[]{:S(2)}) copy-start(f32[2,1024]{1,0:T(2,128)} %gain_ref.1) | copy-start | bytes 24580
  0.0 1.2 %copy-start.3 = (f32[1024]{0:T(1024)S(1)}, f32[1024]{0:T(1024)}, u32[]{:S(2)}) copy-start(f32[1024]{0:T(1024)} %param.13) | copy-start | bytes 12292
  0.0 1.2 %copy-start.4 = (f32[2,512]{1,0:T(2,128)S(1)}, f32[2,512]{1,0:T(2,128)}, u32[]{:S(2)}) copy-start(f32[2,512]{1,0:T(2,128)} %pscale_ref.1) | copy-start | bytes 12292
  1.1 1.0 %copy-start = (bf16[256,1024]{1,0:T(8,128)(2,1)S(1)}, bf16[256,1024]{1,0:T(8,128)(2,1)}, u32[]{:S(2)}) copy-start(bf16[256,1024]{1,0:T(8,128)(2,1)} %resid_ref.1) | copy-start | bytes 1572868
  1.1 1.2 %copy-start.1 = (bf16[2,2,256,256]{3,2,1,0:T(8,128)(2,1)S(1)}, bf16[2,2,256,256]{3,2,1,0:T(8,128)(2,1)}, u32[]{:S(2)}) copy-start(bf16[2,2,256,256]{3,2,1,0:T(8,128)(2,1)} %pool_ref.1) | copy-start | bytes 1572868
